TPU v7x, 32 devices: a whole 2x2x4 slice. The times are simulated.
32 devices in a mesh: sp: 8 (over z, x), tp: 4 (over y, core).
Axes of the slice: x: 2, y: 2, z: 4, core: 2. Of those that a mesh axis runs over, the one named last changes fastest.
Arguments:
- query_rows: bfloat16 [4096, 1024], P('sp', 'tp'), may hold values from -6 to 6
- key_rows: bfloat16 [4096, 1024], P('sp', 'tp'), may hold values from -6 to 6
- value_rows: bfloat16 [4096, 2048], P('sp', 'tp'), may hold values from -6 to 6
- out_gate_pre: bfloat16 [4096, 2048], P('sp', 'tp'), may hold values from -8 to 8
- input_gate_pre: float32 [4, 4096], P('tp', 'sp'), may hold values from -8 to 8
- forget_gate_pre: float32 [4, 4096], P('tp', 'sp'), may hold values from -26 to 26
- residual: bfloat16 [4096, 2048], P(('sp', 'tp')), may hold values from -6 to 6
- out_proj: bfloat16 [2048, 2048], P('tp'), may hold values from -0.125 to 0.125
- mix_gain: float32 [2048], replicated, may hold values from 0.1 to 1.9
- pre_gain: float32 [2048], replicated, may hold values from 0.1 to 1.9
- gate_proj: bfloat16 [2048, 3072], P('sp', 'tp'), may hold values from -0.125 to 0.125
- value_proj: bfloat16 [2048, 3072], P('sp', 'tp'), may hold values from -0.125 to 0.125
- gate_kernel: float32 [3, 3072], P(None, 'tp'), may hold values from -3.5 to 3.5
- value_kernel: float32 [3, 3072], P(None, 'tp'), may hold values from -3.5 to 3.5
- down_proj: bfloat16 [2048, 3072], P('sp', 'tp'), may hold values from -0.109375 to 0.109375
- post_gain: float32 [2048], replicated, may hold values from 0.1 to 1.9
Outputs:
- result: bfloat16 [4096, 2048], P(('sp', 'tp'))
All inputs are finite; a program needn't handle non-finite values.
Results may differ from a plain program's by a relative error of at most 0.017.
Values may be sent and summed in bfloat16 or wider, within the bound.
A program may use at most 128 MiB of HBM per device.

v0:
```python
import jax
import jax.numpy as jnp
from jax import lax
from jax.sharding import PartitionSpec as P

QK = 256
HV = 512
BLOCK = 64
CONV = 3


gate_cap = 15.0
epsilon = 1e-06
highest = lax.Precision.HIGHEST
far_below = -1e30


def prefix(part, axis, combine, identity):
    place = lax.axis_index(axis)
    gathered = jax.tree.map(lambda a: lax.all_gather(a, axis), part)
    state = jax.tree.map(lambda a, e: jnp.zeros_like(a) + jnp.asarray(e, a.dtype), part, identity)

    def one(step, state):
        return combine(
            state, jax.tree.map(lambda a: lax.dynamic_index_in_dim(a, step, 0, False), gathered)
        )

    return lax.fori_loop(0, place, one, state)


def passed_along(block, axis, distance):
    devices = range(lax.axis_size(axis))
    route = [(i - distance, i) for i in devices if i - distance in devices]
    return lax.ppermute(block, axis, route)


def softcap(values):
    return gate_cap * jnp.tanh(values / gate_cap)


def normalize(values, gains):
    return values * lax.rsqrt(jnp.mean(values * values, axis=-1, keepdims=True) + epsilon) * gains


def combine(previous, following):
    prev_total, prev_max, prev_memory, prev_normer = previous
    next_total, next_max, next_memory, next_normer = following
    new_max = jnp.maximum(next_total + prev_max, next_max)
    prev_scale = jnp.exp(next_total + prev_max - new_max)
    next_scale = jnp.exp(next_max - new_max)
    memory = prev_scale[..., None, None] * prev_memory + next_scale[..., None, None] * next_memory
    normer = prev_scale[..., None] * prev_normer + next_scale[..., None] * next_normer
    return (prev_total + next_total, new_max, memory, normer)


def depthwise(padded, kernel, length):
    summed = kernel[0] * padded[0:length]
    for offset in range(1, CONV):
        summed = summed + kernel[offset] * padded[offset : offset + length]
    return summed


def body(
    query_rows,
    key_rows,
    value_rows,
    out_gate_pre,
    input_gate_pre,
    forget_gate_pre,
    residual,
    out_proj,
    mix_gain,
    pre_gain,
    gate_proj,
    value_proj,
    gate_kernel,
    value_kernel,
    down_proj,
    post_gain,
):
    row_count = query_rows.shape[0]
    head_count = input_gate_pre.shape[0]
    blocks = row_count // BLOCK
    hidden_width = gate_proj.shape[1]
    query_scale = QK ** (-0.5)
    query_narrow = (
        (query_rows * jnp.bfloat16(query_scale))
        .reshape(blocks, BLOCK, head_count, QK)
        .transpose(2, 0, 1, 3)
    )
    key_narrow = key_rows.reshape(blocks, BLOCK, head_count, QK).transpose(2, 0, 1, 3)
    queries = query_narrow.astype(jnp.float32)
    key_blocks = key_narrow.astype(jnp.float32)
    value_blocks = (
        value_rows.astype(jnp.float32).reshape(blocks, BLOCK, head_count, HV).transpose(2, 0, 1, 3)
    )
    log_input = softcap(input_gate_pre).reshape(head_count, blocks, BLOCK)
    log_forget = jax.nn.log_sigmoid(softcap(forget_gate_pre)).reshape(head_count, blocks, BLOCK)
    running = jnp.cumsum(log_forget, axis=2)
    block_total = running[..., -1]
    lead_logs = block_total[..., None] - running + log_input
    lead_max = jnp.max(lead_logs, axis=2)
    weighted = key_blocks * jnp.exp(lead_logs - lead_max[..., None])[..., None]
    block_memory = jnp.einsum("hbsd,hbsv->hbdv", weighted, value_blocks, precision=highest)
    segments = (block_total, lead_max, block_memory, jnp.sum(weighted, axis=2))
    inclusive = lax.associative_scan(combine, segments, axis=1)
    summary = tuple((member[:, -1] for member in inclusive))
    identity = (
        jnp.zeros((head_count,), jnp.float32),
        jnp.full((head_count,), far_below, jnp.float32),
        jnp.zeros((head_count, QK, HV), jnp.float32),
        jnp.zeros((head_count, QK), jnp.float32),
    )
    incoming = prefix(summary, "sp", combine, identity)
    exclusive = tuple(
        (
            jnp.concatenate((start_member[:, None], member[:, :-1]), axis=1)
            for start_member, member in zip(identity, inclusive)
        )
    )
    entering = combine(tuple((member[:, None] for member in incoming)), exclusive)
    causal = jnp.tril(jnp.ones((BLOCK, BLOCK), dtype=bool))
    log_weights = jnp.where(
        causal, running[..., :, None] - running[..., None, :] + log_input[..., None, :], -jnp.inf
    )
    carried = running + entering[1][..., None]
    row_max = jnp.maximum(carried, jnp.max(log_weights, axis=3))
    inner_weights = jnp.exp(log_weights - row_max[..., None])
    outer_weights = jnp.exp(carried - row_max)
    scores = (
        jnp.einsum("hbtd,hbsd->hbts", query_narrow, key_narrow, preferred_element_type=jnp.float32)
        * inner_weights
    )
    numerator = outer_weights[..., None] * jnp.einsum(
        "hbtd,hbdv->hbtv", queries, entering[2], precision=highest
    ) + jnp.einsum("hbts,hbsv->hbtv", scores, value_blocks, precision=highest)
    denominator = outer_weights * jnp.einsum(
        "hbtd,hbd->hbt", queries, entering[3], precision=highest
    ) + jnp.sum(scores, axis=3)
    cell_rows = numerator / jnp.maximum(jnp.abs(denominator), jnp.exp(-row_max))[..., None]
    cell_rows = cell_rows.transpose(1, 2, 0, 3).reshape(row_count, head_count * HV)
    gated = (cell_rows * jax.nn.sigmoid(out_gate_pre.astype(jnp.float32))).astype(jnp.bfloat16)
    mixed = lax.psum_scatter(
        jnp.dot(gated, out_proj, preferred_element_type=jnp.float32).astype(jnp.bfloat16),
        "tp",
        scatter_dimension=0,
        tiled=True,
    )
    stream = (residual.astype(jnp.float32) + normalize(mixed.astype(jnp.float32), mix_gain)).astype(
        jnp.bfloat16
    )
    normed = normalize(stream.astype(jnp.float32), pre_gain).astype(jnp.bfloat16)
    gathered = lax.all_gather(normed, "tp", axis=0, tiled=True)
    gate_sum = jnp.dot(
        gathered,
        lax.all_gather(gate_proj, "sp", axis=0, tiled=True),
        preferred_element_type=jnp.float32,
    )
    value_sum = jnp.dot(
        gathered,
        lax.all_gather(value_proj, "sp", axis=0, tiled=True),
        preferred_element_type=jnp.float32,
    )
    up_gate = gate_sum.astype(jnp.bfloat16)
    up_value = value_sum.astype(jnp.bfloat16)
    last_rows = jnp.concatenate(
        (up_gate[row_count - CONV + 1 :], up_value[row_count - CONV + 1 :]), axis=1
    )
    before = passed_along(last_rows, "sp", 1)
    gate_padded = jnp.concatenate((before[:, :hidden_width], up_gate), axis=0).astype(jnp.float32)
    value_padded = jnp.concatenate((before[:, hidden_width:], up_value), axis=0).astype(jnp.float32)
    conv_gate = depthwise(gate_padded, gate_kernel, row_count)
    conv_value = depthwise(value_padded, value_kernel, row_count)
    hidden = (jax.nn.silu(conv_gate) * conv_value).astype(jnp.bfloat16)
    terms = lax.dot_general(
        hidden,
        lax.all_gather(down_proj, "sp", axis=0, tiled=True),
        (((1,), (1,)), ((), ())),
        preferred_element_type=jnp.float32,
    )
    ffn = lax.psum_scatter(terms.astype(jnp.bfloat16), "tp", scatter_dimension=0, tiled=True)
    return (stream.astype(jnp.float32) + normalize(ffn.astype(jnp.float32), post_gain)).astype(
        jnp.bfloat16
    )


def solution(mesh):
    return jax.shard_map(
        body,
        mesh=mesh,
        in_specs=(
            P("sp", "tp"),
            P("sp", "tp"),
            P("sp", "tp"),
            P("sp", "tp"),
            P("tp", "sp"),
            P("tp", "sp"),
            P(("sp", "tp"), None),
            P("tp", None),
            P(),
            P(),
            P("sp", "tp"),
            P("sp", "tp"),
            P(None, "tp"),
            P(None, "tp"),
            P("sp", "tp"),
            P(),
        ),
        out_specs=P(("sp", "tp"), None),
        check_vma=False,
    )
```

profile of v0, /device:TPU:0, one launch (start us, length us, event | category | flops | bytes accessed | tf_op | source)
XLA Modules:
  0.0 458.3 jit_solution(11434014777517902157)
XLA Ops:
  8.6 1.3 fusion.62
  22.7 3.3 convolution_bitcast_fusion
  26.7 1.3 copy-done.1
  29.7 3.5 pad.92
  33.2 2.3 pad.93
  35.5 4.1 add.371
  39.6 5.8 %pad.206 = f32[1,8,256,512]{3,2,1,0:T(8,128)} pad(f32[1,4,256,512]{3,2,1,0:T(8,128)} %add.371, f32[]{:T(128)} %constant.83.clone.1), padding=0_0_0x1_0_1x0_0_0x0_0_0 | pad | bytes 6291460
  45.3 3.0 fusion.15
  48.3 1.6 pad_maximum_fusion
  49.9 5.7 %pad.94 = f32[1,8,256,512]{3,2,1,0:T(8,128)} pad(f32[1,4,256,512]{3,2,1,0:T(8,128)} %pad_maximum_fusion, f32[]{:T(128)} %constant.83.clone.1), padding=0_0_0x0_1_1x0_0_0x0_0_0 | pad | bytes 6291460 | tf_op jit(solution)/shard_map/pad | solution.py:106
  55.6 2.1 slice_add_fusion
  62.7 24.0 %all-reduce.28 = (f32[8]{0:T(128)S(1)}, f32[8]{0:T(128)S(1)}) all-reduce(f32[8]{0:T(128)S(1)} %bitcast_dynamic-update-slice_fusion.1, f32[8]{0:T(128)S(1)} %bitcast_dynamic-update-slice_fusion), channel_id=1, replica_groups=mesh['sp'=8,'tp'=4] {'sp'}, use_global_device_ids=true, to_apply=%add.26 | all-reduce | flops 16 | bytes 128
  87.5 5.7 %pad.132 = f32[1,7,256,512]{3,2,1,0:T(8,128)} pad(f32[1,4,256,512]{3,2,1,0:T(8,128)} %pad_maximum_fusion, f32[]{:T(128)} %constant.83.clone.1), padding=0_0_0x0_0_1x0_0_0x0_0_0 | pad | bytes 5767172 | tf_op jit(solution)/shard_map/slice | solution.py:117
  93.3 17.0 %all_gather.27 = f32[8,1,256]{2,1,0:T(1,128)S(1)} all-gather(f32[1,1,256]{2,1,0:T(1,128)S(1)} %slice_add_fusion.1), channel_id=1, replica_groups=mesh['sp'=8,'tp'=4] {'sp'}, dimensions={0}, use_global_device_ids=true | all-gather | bytes 9216 | tf_op jit(solution)/shard_map/all_gather | solution.py:20
  110.6 5.9 %slice_add_fusion.4 = f32[1,7,256,512]{3,2,1,0:T(8,128)} fusion(f32[1,7,256,512]{3,2,1,0:T(8,128)} %pad.132, f32[1,8,256,512]{3,2,1,0:T(8,128)} %pad.206), kind=kLoop, calls=%fused_computation.162 | loop fusion | flops 917504 | bytes 11010048 | tf_op jit(solution)/shard_map/add | solution.py:106
  116.5 17.3 %all-gather.6.cloned.1.call-done = f32[8,1,256,512]{3,2,1,0:T(8,128)} async-done(((f32[1,1,256,512]{3,2,1,0:T(8,128)}), f32[8,1,256,512]{3,2,1,0:T(8,128)}) %all-gather.6.cloned.1.call-update) | async-done | bytes 4194320 | tf_op jit(solution)/shard_map/all_gather | solution.py:20
  135.0 4.3 fusion.17
  140.7 2.6 convolution_convert_fusion.1
  144.1 57.3 %reduce-scatter.3.cloned.1.call-done = bf16[128,2048]{1,0:T(8,128)(2,1)} async-done(((bf16[512,2048]{1,0:T(8,128)(2,1)}), bf16[128,2048]{1,0:T(8,128)(2,1)}) %reduce-scatter.3.cloned.1.call-update) | async-done | bytes 524304 | tf_op jit(solution)/shard_map/reduce_scatter | solution.py:143
  202.6 1.4 fusion.26
  206.3 57.3 %all-gather.10.cloned.1.call-done = bf16[2048,768]{1,0:T(8,128)(2,1)} async-done(((bf16[256,768]{1,0:T(8,128)(2,1)}), bf16[2048,768]{1,0:T(8,128)(2,1)}) %all-gather.10.cloned.1.call-update) | async-done | bytes 3145744 | tf_op jit(solution)/shard_map/all_gather | solution.py:156
  263.6 22.7 %all-gather.8.cloned.1.call-done = bf16[512,2048]{1,0:T(8,128)(2,1)} async-done(((bf16[128,2048]{1,0:T(8,128)(2,1)}), bf16[512,2048]{1,0:T(8,128)(2,1)}) %all-gather.8.cloned.1.call-update) | async-done | bytes 2097168 | tf_op jit(solution)/shard_map/all_gather | solution.py:153
  286.3 4.3 convolution_convert_fusion.3
  290.7 57.7 %all-gather.12.cloned.1.call-done = bf16[2048,768]{1,0:T(8,128)(2,1)} async-done(((bf16[256,768]{1,0:T(8,128)(2,1)}), bf16[2048,768]{1,0:T(8,128)(2,1)}) %all-gather.12.cloned.1.call-update) | async-done | bytes 3145744 | tf_op jit(solution)/shard_map/all_gather | solution.py:161
  348.4 4.3 convolution_convert_fusion.2
  352.7 2.5 collective-permute-start
  356.5 1.3 maximum_convert_fusion
  357.8 1.4 maximum_convert_fusion.1
  359.2 49.9 %all-gather.14.cloned.1.call-done = bf16[2048,768]{1,0:T(8,128)(2,1)} async-done(((bf16[256,768]{1,0:T(8,128)(2,1)}), bf16[2048,768]{1,0:T(8,128)(2,1)}) %all-gather.14.cloned.1.call-update) | async-done | bytes 3145744 | tf_op jit(solution)/shard_map/all_gather | solution.py:177
  409.1 9.0 %convolution_convert_fusion = bf16[512,2048]{1,0:T(8,128)(2,1)} fusion(bf16[2048,768]{1,0:T(8,128)(2,1)} %all-gather.14.cloned.1.call-done, f32[514,768]{1,0:T(8,128)} %maximum_convert_fusion.1, f32[514,768]{1,0:T(8,128)} %maximum_convert_fusion, f32[768]{0:T(1024)S(1)} %get-tuple-element.86, f32[768]{0:T(1024)S(1)} %get-tuple-element.87, ...), kind=kOutput, calls=%fused_computation.10 | convolution fusion | flops 1617952768 | bytes 14698496 | tf_op jit(solution)/shard_map/dot_general | solution.py:175
  418.1 30.0 %reduce-scatter.5.cloned.1.call-done = bf16[128,2048]{1,0:T(8,128)(2,1)} async-done(((bf16[512,2048]{1,0:T(8,128)(2,1)}), bf16[128,2048]{1,0:T(8,128)(2,1)}) %reduce-scatter.5.cloned.1.call-update) | async-done | bytes 524304 | tf_op jit(solution)/shard_map/reduce_scatter | solution.py:181
  449.4 2.1 fusion.29
  (155 shorter events, 25.9 us)
Async XLA Ops:
  6.5 134.1 %copy-start = (bf16[512,2048]{1,0:T(8,128)(2,1)S(1)}, bf16[512,2048]{1,0:T(8,128)(2,1)}, u32[]{:S(2)}) copy-start(bf16[512,2048]{1,0:T(8,128)(2,1)} %param.25) | copy-start | bytes 6291460
  6.5 127.3 %all-gather.6.cloned.1.call-start = ((), (), s32[]{:S(2)}) async-start(), calls=%async_computation.2 | async-start | bytes 4718592 | tf_op jit(solution)/shard_map/all_gather | solution.py:20
  26.1 1.9 copy-start.1
  45.3 3.0 slice-start
  55.6 4.0 copy-start.12
  55.6 31.2 %copy-start.2 = (bf16[512,256]{1,0:T(8,128)(2,1)S(1)}, bf16[512,256]{1,0:T(8,128)(2,1)}, u32[]{:S(2)}) copy-start(bf16[512,256]{1,0:T(8,128)(2,1)} %param.19) | copy-start | bytes 786436
  57.7 143.6 %reduce-scatter.3.cloned.1.call-start = ((), (), s32[]{:S(2)}) async-start(), calls=%async_computation.3 | async-start | bytes 2621440 | tf_op jit(solution)/shard_map/reduce_scatter | solution.py:143
  87.5 23.0 %copy-start.6 = (bf16[512,256]{1,0:T(8,128)(2,1)S(1)}, bf16[512,256]{1,0:T(8,128)(2,1)}, u32[]{:S(2)}) copy-start(bf16[512,256]{1,0:T(8,128)(2,1)} %param.18) | copy-start | bytes 786436
  135.0 4.3 copy-start.5
  139.3 1.0 copy-start.3
  143.3 59.3 %copy-start.4 = (bf16[128,2048]{1,0:T(8,128)(2,1)S(1)}, bf16[128,2048]{1,0:T(8,128)(2,1)}, u32[]{:S(2)}) copy-start(bf16[128,2048]{1,0:T(8,128)(2,1)} %param.24) | copy-start | bytes 1572868
  143.3 59.3 %copy-start.7 = (f32[2048]{0:T(1024)S(1)}, f32[2048]{0:T(1024)}, u32[]{:S(2)}) copy-start(f32[2048]{0:T(1024)} %param.26) | copy-start | bytes 24580
  143.3 60.8 %copy-start.8 = (f32[2048]{0:T(1024)S(1)}, f32[2048]{0:T(1024)}, u32[]{:S(2)}) copy-start(f32[2048]{0:T(1024)} %param.27) | copy-start | bytes 24580
  143.3 120.3 %all-gather.10.cloned.1.call-start = ((), (), s32[]{:S(2)}) async-start(), calls=%async_computation.5 | async-start | bytes 3538944 | tf_op jit(solution)/shard_map/all_gather | solution.py:156
  144.0 142.3 %all-gather.8.cloned.1.call-start = ((), (), s32[]{:S(2)}) async-start(), calls=%async_computation.4 | async-start | bytes 2621440 | tf_op jit(solution)/shard_map/all_gather | solution.py:153
  205.1 143.3 %all-gather.12.cloned.1.call-start = ((), (), s32[]{:S(2)}) async-start(), calls=%async_computation.6 | async-start | bytes 3538944 | tf_op jit(solution)/shard_map/all_gather | solution.py:161
  205.7 203.4 %all-gather.14.cloned.1.call-start = ((), (), s32[]{:S(2)}) async-start(), calls=%async_computation.7 | async-start | bytes 3538944 | tf_op jit(solution)/shard_map/all_gather | solution.py:177
  206.3 241.9 %reduce-scatter.5.cloned.1.call-start = ((), (), s32[]{:S(2)}) async-start(), calls=%async_computation.8 | async-start | bytes 2621440 | tf_op jit(solution)/shard_map/reduce_scatter | solution.py:181
  290.6 64.6 %copy-start.10 = (f32[3,768]{1,0:T(4,128)S(1)}, f32[3,768]{1,0:T(4,128)}, u32[]{:S(2)}) copy-start(f32[3,768]{1,0:T(4,128)} %param.31) | copy-start | bytes 27652
  290.6 64.6 %copy-start.11 = (f32[3,768]{1,0:T(4,128)S(1)}, f32[3,768]{1,0:T(4,128)}, u32[]{:S(2)}) copy-start(f32[3,768]{1,0:T(4,128)} %param.30) | copy-start | bytes 27652
  352.7 3.8 collective-permute-start
  418.1 31.3 %copy-start.9 = (f32[2048]{0:T(1024)S(1)}, f32[2048]{0:T(1024)}, u32[]{:S(2)}) copy-start(f32[2048]{0:T(1024)} %param.33) | copy-start | bytes 24580
Sparse Core Ops, SparseCore 0:
  57.9 75.8 all-gather.5
  143.4 57.9 reduce-scatter.2
  203.6 60.0 all-gather.9
  265.0 21.2 all-gather.7
  288.3 59.9 all-gather.11
  350.4 58.6 all-gather.13
  418.3 29.8 reduce-scatter.4
where the time goes:
time: 460 us; the launch traced here: 458 us
  waiting for transfers between devices  295 us (64%)
  blocking collectives  41 us (9%)
  other arithmetic  35.7 us (8%)
  local copies, waits for them, and re-layouts  33.9 us (7%)
  matrix products  29.1 us (6%)
  between operations  20.5 us (4%)
    all_gather x1, waiting for transfers between devices, body(): lax.all_gather(value_proj, 'sp', axis=0, tiled=True)  57.7 us
    all_gather x1, waiting for transfers between devices, body(): lax.all_gather(gate_proj, 'sp', axis=0, tiled=True)  57.3 us
    reduce_scatter x1, waiting for transfers between devices, body(): lax.psum_scatter(jnp.dot(gated, out_proj, preferred_element_type=jnp.floa...  57.3 us
    all_gather x1, waiting for transfers between devices, body(): lax.all_gather(down_proj, 'sp', axis=0, tiled=True)  49.9 us
    reduce_scatter x1, waiting for transfers between devices, body(): lax.psum_scatter(terms.astype(jnp.bfloat16), 'tp', scatter_dimension=0, t...  30 us
    unnamed x1, blocking collectives  24 us
    all_gather x1, waiting for transfers between devices, body(): gathered = lax.all_gather(normed, 'tp', axis=0, tiled=True)  22.7 us
    all_gather x1, waiting for transfers between devices, prefix(): gathered = jax.tree.map(lambda a: lax.all_gather(a, axis), part)  17.3 us
  transfers between devices with their start and end apart: 8, of which 8 were waited for; matrix products, arithmetic and copies ran while one was open for 7% of the time, Pallas kernels for 0%

commit v1 on v0

v1 whole, which is shorter than its diff:
```python
import functools
import jax
import jax.numpy as jnp
from jax import lax
from jax.experimental import pallas as pl
from jax.experimental.pallas import tpu as pltpu
from jax.sharding import PartitionSpec as P

CONV = 3
HALO = 16
gate_cap = 15.0
epsilon = 1e-06
far_below = -1e30
MESH = pl.DeviceIdType.MESH
f32 = jnp.float32
bf16 = jnp.bfloat16


def softcap(values):
    return gate_cap * jnp.tanh(values / gate_cap)


def sigmoid(values):
    return 1.0 / (1.0 + jnp.exp(-values))


def normalize(values, gains):
    return values * lax.rsqrt(jnp.mean(values * values, axis=-1, keepdims=True) + epsilon) * gains


def dot(a, b, ca=1, cb=0):
    return lax.dot_general(a, b, (((ca,), (cb,)), ((), ())), preferred_element_type=f32)


def kernel(
    n, m, owners, chunks,
    q_ref, k_ref, v_ref, og_ref, ig_ref, fg_ref, res_ref, op_ref,
    mg_ref, pg_ref, gp_ref, vp_ref, gk_ref, vk_ref, dp_ref, sg_ref,
    out_ref,
    w_all, st_send, small, slices, pre_send, mem_in,
    gated, mix_send, mix_recv, normed_all, upg, upv, halo_send, halo_recv, hidden, ffn_send, ffn_recv,
    own_sem, z_send, x_send, w_recv, sm_send, sm_recv, sl_send, sl_recv, pr_send, pr_recv,
    mx_send, mx_recv, ag_send, ag_recv, h_send, h_recv, f_send, f_recv,
):
    s = lax.axis_index("sp")
    t = lax.axis_index("tp")
    inner = 2
    zs = n // inner
    x = lax.rem(s, inner)
    z = lax.div(s, inner)
    mate = z * inner + (1 - x)
    rows, qk = q_ref.shape
    block = gp_ref.shape[0]
    width = w_all.shape[1]
    part = rows // m
    piece = qk // owners
    scale = qk ** (-0.5)

    def remote(src, dst, ss, rs, **dev):
        return pltpu.make_async_remote_copy(
            src_ref=src, dst_ref=dst, send_sem=ss, recv_sem=rs, device_id=dev, device_id_type=MESH
        )

    barrier = pltpu.get_barrier_semaphore()
    for d in range(1, n):
        pl.semaphore_signal(barrier, inc=1, device_id={"sp": lax.rem(s + d, n)}, device_id_type=MESH)
    for d in range(1, m):
        pl.semaphore_signal(barrier, inc=1, device_id={"tp": lax.rem(t + d, m)}, device_id_type=MESH)
    pl.semaphore_wait(barrier, n + m - 2)

    def slot(w, blk):
        return w_all.at[w, pl.ds(pl.multiple_of(blk * block, block), block), :]

    waits = []
    own = []
    for w, ref in enumerate((gp_ref, vp_ref, dp_ref)):
        c = pltpu.make_async_copy(ref, slot(w, s), own_sem.at[w])
        c.start()
        own.append(c)
        c = remote(ref, slot(w, s), x_send.at[w, 0], w_recv.at[w, s], sp=mate)
        c.start()
        waits.append(c)
        for d in range(1, zs):
            c = remote(
                ref, slot(w, s), z_send.at[w, d - 1], w_recv.at[w, s],
                sp=lax.rem(z + d, zs) * inner + x,
            )
            c.start()
            waits.append(c)

    def arrived(w, blk):
        remote(slot(w, blk), slot(w, blk), x_send.at[w, 0], w_recv.at[w, blk], sp=mate).wait_recv()

    def relay(w, d):
        blk = lax.rem(z + d, zs) * inner + x
        arrived(w, blk)
        c = remote(slot(w, blk), slot(w, blk), x_send.at[w, d], w_recv.at[w, blk], sp=mate)
        c.start()
        waits.append(c)
        return blk

    def mate_block(d):
        return lax.rem(z + d, zs) * inner + (1 - x)

    i = lax.broadcasted_iota(jnp.int32, (rows, rows), 0)
    j = lax.broadcasted_iota(jnp.int32, (rows, rows), 1)
    li_row = softcap(ig_ref[...])
    fg = softcap(fg_ref[...])
    lf_row = jnp.minimum(fg, 0.0) - jnp.log1p(jnp.exp(-jnp.abs(fg)))
    run_col = jnp.sum(jnp.where(j <= i, lf_row, 0.0), axis=1, keepdims=True)
    run_row = jnp.sum(jnp.where(j == i, run_col, 0.0), axis=0, keepdims=True)
    li_col = jnp.sum(jnp.where(j == i, li_row, 0.0), axis=1, keepdims=True)
    total = run_col[rows - 1 : rows, :]
    lead = total - run_col + li_col
    lead_max = jnp.max(lead, axis=0, keepdims=True)
    weighted = k_ref[...].astype(f32) * jnp.exp(lead - lead_max)
    norm_row = jnp.sum(weighted, axis=0, keepdims=True)
    st_send[...] = dot(weighted.astype(bf16), v_ref[...], 0, 0).astype(bf16)
    r8 = lax.broadcasted_iota(jnp.int32, (8, qk), 0)
    small[s] = jnp.where(r8 == 0, norm_row, jnp.where(r8 == 1, total, lead_max))

    def only_owner(who, fn):
        if owners == n:
            fn()
        else:
            pl.when(who < owners)(fn)

    def rows_of(r):
        return pl.ds(pl.multiple_of(r * piece, piece), piece)

    for d in range(1, n):
        to = lax.rem(s + d, n)
        c = remote(small.at[s], small.at[s], sm_send.at[d - 1], sm_recv.at[s], sp=to)
        c.start()
        waits.append(c)

        def send_slice(d=d, to=to):
            remote(
                st_send.at[rows_of(to), :], slices.at[s], sl_send.at[d - 1], sl_recv.at[s], sp=to
            ).start()

        only_owner(to, send_slice)

    def keep_slice():
        slices[s] = st_send[rows_of(s), :]

    only_owner(s, keep_slice)

    log_w = jnp.where(j <= i, run_col - run_row + li_row, far_below)
    loc_max = jnp.max(log_w, axis=1, keepdims=True)
    scores = dot(q_ref[...], k_ref[...], 1, 1) * scale * jnp.exp(log_w - loc_max)
    den_loc = jnp.sum(scores, axis=1, keepdims=True)
    num_loc = dot(scores.astype(bf16), v_ref[...])

    for d in range(1, n):
        src = lax.rem(s + d, n)
        remote(small.at[src], small.at[src], sm_send.at[0], sm_recv.at[src], sp=src).wait_recv()

    def step_small(a, carry):
        top, nrm = carry
        tile = small[a]
        nt = tile[1:2, 0:1] + top
        new = jnp.maximum(nt, tile[2:3, 0:1])
        upd = jnp.exp(nt - new) * nrm + jnp.exp(tile[2:3, 0:1] - new) * tile[0:1, :]
        live = a < s
        return jnp.where(live, new, top), jnp.where(live, upd, nrm)

    def step_mem(a, carry):
        top, mem = carry
        tile = small[a]
        nt = tile[1:2, 0:1] + top
        new = jnp.maximum(nt, tile[2:3, 0:1])
        mem = jnp.exp(nt - new) * mem + jnp.exp(tile[2:3, 0:1] - new) * slices[a].astype(f32)
        pre_send[a + 1] = mem.astype(bf16)
        return new, mem

    def steps(count, fn, carry):
        if count <= 8:
            for a in range(count):
                carry = fn(a, carry)
            return carry
        return lax.fori_loop(0, count, fn, carry)

    start_max = jnp.full((1, 1), far_below, f32)
    m_in, n_in = steps(n - 1, step_small, (start_max, jnp.zeros((1, qk), f32)))

    def own_prefixes():
        for d in range(1, n):
            src = lax.rem(s + d, n)
            remote(
                slices.at[src], slices.at[src], sl_send.at[0], sl_recv.at[src], sp=src
            ).wait_recv()
        pre_send[0] = jnp.zeros(pre_send.shape[1:], bf16)
        steps(n - 1, step_mem, (start_max, jnp.zeros(pre_send.shape[1:], f32)))
        for d in range(1, n):
            to = lax.rem(s + d, n)
            remote(
                pre_send.at[to], mem_in.at[rows_of(s), :], pr_send.at[d - 1], pr_recv.at[s], sp=to
            ).start()
        mem_in[rows_of(s), :] = pre_send[s]

    only_owner(s, own_prefixes)
    for d in range(1, n):
        src = lax.rem(s + d, n)

        def got(src=src):
            remote(
                mem_in.at[rows_of(src), :], mem_in.at[rows_of(src), :],
                pr_send.at[0], pr_recv.at[src], sp=src,
            ).wait_recv()

        only_owner(src, got)

    carried = run_col + m_in
    top = jnp.maximum(carried, loc_max)
    inner_w = jnp.exp(loc_max - top)
    outer_w = jnp.exp(carried - top) * scale
    num = inner_w * num_loc + outer_w * dot(q_ref[...], mem_in[...])
    den = inner_w * den_loc + outer_w * jnp.sum(
        q_ref[...].astype(f32) * n_in, axis=1, keepdims=True
    )
    cell = num / jnp.maximum(jnp.abs(den), jnp.exp(-top))
    gated[...] = (cell * sigmoid(og_ref[...].astype(f32))).astype(bf16)

    def part_of(a):
        return pl.ds(pl.multiple_of(a * part, part), part)

    for d in range(1, m):
        to = lax.rem(t + d, m)
        mix_send[d - 1] = dot(gated[part_of(to), :], op_ref[...]).astype(bf16)
        c = remote(mix_send.at[d - 1], mix_recv.at[d - 1], mx_send.at[d - 1], mx_recv.at[d - 1], tp=to)
        c.start()
        waits.append(c)
    mixed = dot(gated[part_of(t), :], op_ref[...]).astype(bf16).astype(f32)
    for d in range(1, zs):
        relay(0, d)
    for d in range(1, m):
        remote(
            mix_send.at[d - 1], mix_recv.at[d - 1], mx_send.at[d - 1], mx_recv.at[d - 1], tp=t
        ).wait_recv()
        mixed = mixed + mix_recv[d - 1].astype(f32)
    mixed = mixed.astype(bf16).astype(f32)
    stream = (res_ref[...].astype(f32) + normalize(mixed, mg_ref[...])).astype(bf16)
    out_ref[...] = stream
    normed_all[part_of(t), :] = normalize(stream.astype(f32), pg_ref[...]).astype(bf16)
    for d in range(1, m):
        to = lax.rem(t + d, m)
        c = remote(
            normed_all.at[part_of(t), :], normed_all.at[part_of(t), :],
            ag_send.at[d - 1], ag_recv.at[t], tp=to,
        )
        c.start()
        waits.append(c)
    for d in range(1, zs):
        relay(1, d)
    own[0].wait()
    own[1].wait()
    for w in range(2):
        for d in range(zs):
            arrived(w, mate_block(d))
    for d in range(1, m):
        src = lax.rem(t + d, m)
        remote(
            normed_all.at[part_of(src), :], normed_all.at[part_of(src), :],
            ag_send.at[0], ag_recv.at[src], tp=src,
        ).wait_recv()

    hid = upg.shape[1]
    cols = 256 if hid % 256 == 0 else 128
    for w, ref in ((0, upg), (1, upv)):

        def up_cols(a, _, w=w, ref=ref):
            cs = pl.ds(pl.multiple_of(a * cols, cols), cols)
            ref[pl.ds(HALO, rows), cs] = dot(normed_all[...], w_all[w, :, cs]).astype(bf16)
            return 0

        lax.fori_loop(0, hid // cols, up_cols, 0)
        halo_send[w] = ref[pl.ds(rows, HALO), :]

    halo = remote(halo_send, halo_recv, h_send, h_recv, sp=lax.rem(s + 1, n))

    @pl.when(s < n - 1)
    def _():
        halo.start()

    @pl.when(s == 0)
    def _():
        upg[pl.ds(0, HALO), :] = jnp.zeros((HALO, hid), bf16)
        upv[pl.ds(0, HALO), :] = jnp.zeros((HALO, hid), bf16)

    @pl.when(s > 0)
    def _():
        halo.wait_recv()
        upg[pl.ds(0, HALO), :] = halo_recv[0]
        upv[pl.ds(0, HALO), :] = halo_recv[1]

    def conv(ref, kern, r0, cs):
        u = ref[pl.ds(r0, part + HALO), cs].astype(f32)
        total_ = kern[CONV - 1 : CONV, cs] * u
        for back in range(1, CONV):
            total_ = total_ + kern[CONV - 1 - back : CONV - back, cs] * pltpu.roll(u, back, 0)
        return total_[HALO:, :]

    def conv_rows(a, _):
        r0 = pl.multiple_of(a * part, part)
        for c0 in range(0, hid, cols):
            cs = pl.ds(c0, cols)
            g = conv(upg, gk_ref, r0, cs)
            u = conv(upv, vk_ref, r0, cs)
            hidden[pl.ds(r0, part), cs] = (g / (1.0 + jnp.exp(-g)) * u).astype(bf16)
        return 0

    lax.fori_loop(0, rows // part, conv_rows, 0)

    feats = width // chunks

    def chunk(c, kth):
        fs = pl.ds(pl.multiple_of(c * feats, feats), feats)
        ffn_send[:, fs] = dot(hidden[...], w_all[2, fs, :], 1, 1).astype(bf16)
        for d in range(1, m):
            to = lax.rem(t + d, m)
            cp = remote(
                ffn_send.at[part_of(to), fs], ffn_recv.at[d - 1, :, fs],
                f_send.at[d - 1, kth], f_recv.at[d - 1, c], tp=to,
            )
            cp.start()
            waits.append(cp)

    own[2].wait()
    if chunks == n:
        chunk(s, 0)
        for d in range(1, zs):
            chunk(relay(2, d), d)
        for d in range(zs):
            blk = mate_block(d)
            arrived(2, blk)
            chunk(blk, zs + d)
    else:
        for d in range(1, zs):
            relay(2, d)
        for d in range(zs):
            arrived(2, mate_block(d))
        for c in range(chunks):
            chunk(c, c)

    for c in range(chunks):
        fs = pl.ds(c * feats, feats)
        for d in range(1, m):
            remote(
                ffn_send.at[part_of(t), fs], ffn_recv.at[d - 1, :, fs],
                f_send.at[d - 1, 0], f_recv.at[d - 1, c], tp=t,
            ).wait_recv()
    ffn = ffn_send[part_of(t), :].astype(f32)
    for d in range(1, m):
        ffn = ffn + ffn_recv[d - 1].astype(f32)
    ffn = ffn.astype(bf16).astype(f32)
    out_ref[...] = (out_ref[...].astype(f32) + normalize(ffn, sg_ref[...])).astype(bf16)

    for c in waits:
        c.wait_send()
    for d in range(1, n):
        to = lax.rem(s + d, n)

        def done_slice(d=d, to=to):
            remote(
                st_send.at[rows_of(to), :], slices.at[s], sl_send.at[d - 1], sl_recv.at[s], sp=to
            ).wait_send()

        only_owner(to, done_slice)

    def done_prefix():
        for d in range(1, n):
            to = lax.rem(s + d, n)
            remote(
                pre_send.at[to], mem_in.at[rows_of(s), :], pr_send.at[d - 1], pr_recv.at[s], sp=to
            ).wait_send()

    only_owner(s, done_prefix)

    @pl.when(s < n - 1)
    def _():
        halo.wait_send()


def body(
    n, m,
    query_rows, key_rows, value_rows, out_gate_pre, input_gate_pre, forget_gate_pre,
    residual, out_proj, mix_gain, pre_gain, gate_proj, value_proj, gate_kernel, value_kernel,
    down_proj, post_gain,
):
    rows, qk = query_rows.shape
    hv = value_rows.shape[1]
    width = residual.shape[1]
    block, hid = gate_proj.shape
    part = rows // m
    owners = min(n, qk // 32)
    chunks = min(n, width // 256)
    dma = pltpu.SemaphoreType.DMA
    vm = pl.BlockSpec(memory_space=pltpu.VMEM)
    hbm = pl.BlockSpec(memory_space=pl.ANY)
    zs = n // 2
    return pl.pallas_call(
        functools.partial(kernel, n, m, owners, chunks),
        out_shape=jax.ShapeDtypeStruct(residual.shape, bf16),
        in_specs=[vm] * 10 + [hbm, hbm, vm, vm, hbm, vm],
        out_specs=vm,
        scratch_shapes=[
            pltpu.VMEM((3, width, hid), bf16),
            pltpu.VMEM((qk, hv), bf16),
            pltpu.VMEM((n, 8, qk), f32),
            pltpu.VMEM((n, qk // owners, hv), bf16),
            pltpu.VMEM((n, qk // owners, hv), bf16),
            pltpu.VMEM((qk, hv), bf16),
            pltpu.VMEM((rows, hv), bf16),
            pltpu.VMEM((m - 1, part, width), bf16),
            pltpu.VMEM((m - 1, part, width), bf16),
            pltpu.VMEM((rows, width), bf16),
            pltpu.VMEM((HALO + rows, hid), bf16),
            pltpu.VMEM((HALO + rows, hid), bf16),
            pltpu.VMEM((2, HALO, hid), bf16),
            pltpu.VMEM((2, HALO, hid), bf16),
            pltpu.VMEM((rows, hid), bf16),
            pltpu.VMEM((rows, width), bf16),
            pltpu.VMEM((m - 1, part, width), bf16),
            dma((3,)),
            dma((3, zs)),
            dma((3, zs)),
            dma((3, n)),
            dma((n,)),
            dma((n,)),
            dma((n,)),
            dma((n,)),
            dma((n,)),
            dma((n,)),
            dma((m,)),
            dma((m,)),
            dma((m,)),
            dma((m,)),
            dma,
            dma,
            dma((m, chunks)),
            dma((m, chunks)),
        ],
        compiler_params=pltpu.CompilerParams(
            collective_id=0, has_side_effects=True, vmem_limit_bytes=64000000
        ),
        name="layer",
    )(
        query_rows, key_rows, value_rows, out_gate_pre, input_gate_pre, forget_gate_pre,
        residual, out_proj, mix_gain.reshape(1, -1), pre_gain.reshape(1, -1),
        gate_proj, value_proj, gate_kernel, value_kernel, down_proj, post_gain.reshape(1, -1),
    )


def solution(mesh):
    return jax.shard_map(
        functools.partial(body, mesh.shape["sp"], mesh.shape["tp"]),
        mesh=mesh,
        in_specs=(
            P("sp", "tp"),
            P("sp", "tp"),
            P("sp", "tp"),
            P("sp", "tp"),
            P("tp", "sp"),
            P("tp", "sp"),
            P(("sp", "tp"), None),
            P("tp", None),
            P(),
            P(),
            P("sp", "tp"),
            P("sp", "tp"),
            P(None, "tp"),
            P(None, "tp"),
            P("sp", "tp"),
            P(),
        ),
        out_specs=P(("sp", "tp"), None),
        check_vma=False,
    )
```

time: 460 us -> 222 us (0.48)
  waiting for transfers between devices: 295 us -> 0 us
  Pallas kernels: 0 us -> 217 us
  blocking collectives: 41 us -> 0 us
  other arithmetic: 35.7 us -> 0 us
  local copies, waits for them, and re-layouts: 33.9 us -> 1.88 us
  matrix products: 29.1 us -> 0 us
  between operations: 20.5 us -> 0.01 us
    pallas_call x0 -> x1, Pallas kernels: none -> 217 us  [body(): pl.pallas_call(functools.partial(kernel, n, m, owners, chunks), out_shape...]
    all_gather x5 -> x0, waiting for transfers between devices: 205 us -> none  [the longest x1 57.7 us: body(): lax.all_gather(value_proj, 'sp', axis=0, tiled=True)]
    reduce_scatter x2 -> x0, waiting for transfers between devices: 87.3 us -> none  [the longest x1 57.3 us: body(): lax.psum_scatter(jnp.dot(gated, out_proj, preferred_element_type=jnp.floa...]
    dot_general x9 -> x0, matrix products: 29.1 us -> none  [the longest x1 8.99 us: body(): lax.dot_general(hidden, lax.all_gather(down_proj, 'sp', axis=0, tiled=Tru...]
    unnamed x1 -> x0, blocking collectives: 24 us -> none
    add x23 -> x0, other arithmetic: 17.8 us -> none  [the longest x14 13.6 us: body(): inclusive = lax.associative_scan(combine, segments, axis=1)]
    all_gather x1 -> x0, blocking collectives: 17 us -> none  [prefix(): gathered = jax.tree.map(lambda a: lax.all_gather(a, axis), part)]
    pad x15 -> x0, local copies, waits for them, and re-layouts: 12.2 us -> none  [body(): inclusive = lax.associative_scan(combine, segments, axis=1)]
  transfers between devices with their start and end apart: 8 -> 0, of which waited for: 8 -> 0; matrix products, arithmetic and copies ran while one was open for 7% -> 0% of each run, Pallas kernels for 0% -> 0%
where the time goes in v1:
time: 222 us; the launch traced here: 219 us
  Pallas kernels  217 us (98%)
    pallas_call x1, Pallas kernels, body(): pl.pallas_call(functools.partial(kernel, n, m, owners, chunks), out_shape...  217 us

profile of v1, /device:TPU:0, one launch (start us, length us, event | category | flops | bytes accessed | tf_op | source)
XLA Modules:
  0.0 219.3 jit_solution(5734556976250339038)
XLA Ops:
  0.0 217.4 %layer.1 = bf16[128,2048]{1,0:T(8,128)(2,1)} custom-call(bf16[512,256]{1,0:T(8,128)(2,1)} %q_ref.1, bf16[512,256]{1,0:T(8,128)(2,1)} %k_ref.1, bf16[512,512]{1,0:T(8,128)(2,1)} %v_ref.1, bf16[512,512]{1,0:T(8,128)(2,1)} %og_ref.1, f32[1,512]{1,0:T(1,128)} %ig_ref.1, f32[1,512]{1,0:T(1,128)} %fg_ref.1, bf16[128,2048]{1,0:T(8,128)(2,1)} %res_ref.1, ...), custom_call_target="tpu_custom_call" | custom-call | tf_op jit(solution)/shard_map/layer/pallas_call | solution.py:402
  217.4 1.9 copy.18

commit v2 on v1

--- a/solution.py
+++ b/solution.py
@@ -38,9 +38,9 @@
     mg_ref, pg_ref, gp_ref, vp_ref, gk_ref, vk_ref, dp_ref, sg_ref,
     out_ref,
     w_all, st_send, small, slices, pre_send, mem_in,
-    gated, mix_send, mix_recv, normed_all, upg, upv, halo_send, halo_recv, hidden, ffn_send, ffn_recv,
+    gated, mix_send, mix_pair, mix_far, mix_recv, normed_all, upg, upv, halo_send, halo_recv, hidden, ffn_send, ffn_pair, ffn_far, ffn_recv,
     own_sem, z_send, x_send, w_recv, sm_send, sm_recv, sl_send, sl_recv, pr_send, pr_recv,
-    mx_send, mx_recv, ag_send, ag_recv, h_send, h_recv, f_send, f_recv,
+    mx_send, mx_recv, my_send, my_recv, ag_send, ag_recv, h_send, h_recv, f_send, f_recv, g_send, g_recv,
 ):
     s = lax.axis_index("sp")
     t = lax.axis_index("tp")
@@ -72,35 +72,60 @@
         return w_all.at[w, pl.ds(pl.multiple_of(blk * block, block), block), :]
 
     waits = []
+    held = []
     own = []
-    for w, ref in enumerate((gp_ref, vp_ref, dp_ref)):
-        c = pltpu.make_async_copy(ref, slot(w, s), own_sem.at[w])
+    refs = (gp_ref, vp_ref, dp_ref)
+    above = jnp.minimum(z + 1, zs - 1) * inner + x
+    below = jnp.maximum(z - 1, 0) * inner + x
+    has_above = z + 1 < zs
+    has_below = z > 0
+
+    def pass_on(w, src, blk, k, cond, to):
+        c = remote(src, slot(w, blk), z_send.at[w, k], w_recv.at[w, blk], sp=to)
+        pl.when(cond)(c.start)
+        held.append((cond, c))
+
+    def send_own(w):
+        pass_on(w, refs[w], s, 0, has_above, above)
+        pass_on(w, refs[w], s, zs, has_below, below)
+        c = remote(refs[w], slot(w, s), x_send.at[w, 0], w_recv.at[w, s], sp=mate)
+        c.start()
+        waits.append(c)
+        c = pltpu.make_async_copy(refs[w], slot(w, s), own_sem.at[w])
         c.start()
         own.append(c)
-        c = remote(ref, slot(w, s), x_send.at[w, 0], w_recv.at[w, s], sp=mate)
-        c.start()
-        waits.append(c)
-        for d in range(1, zs):
-            c = remote(
-                ref, slot(w, s), z_send.at[w, d - 1], w_recv.at[w, s],
-                sp=lax.rem(z + d, zs) * inner + x,
-            )
-            c.start()
-            waits.append(c)
 
     def arrived(w, blk):
         remote(slot(w, blk), slot(w, blk), x_send.at[w, 0], w_recv.at[w, blk], sp=mate).wait_recv()
 
-    def relay(w, d):
-        blk = lax.rem(z + d, zs) * inner + x
-        arrived(w, blk)
-        c = remote(slot(w, blk), slot(w, blk), x_send.at[w, d], w_recv.at[w, blk], sp=mate)
-        c.start()
-        waits.append(c)
-        return blk
-
-    def mate_block(d):
-        return lax.rem(z + d, zs) * inner + (1 - x)
+    def relay_one(w, k, upward):
+        if upward:
+            cond, zz, room, to, base = z >= k, jnp.maximum(z - k, 0), has_above, above, 0
+        else:
+            cond, zz, room, to, base = z + k < zs, jnp.minimum(z + k, zs - 1), has_below, below, zs
+        blk = zz * inner + x
+
+        @pl.when(cond)
+        def _():
+            arrived(w, blk)
+
+        if k < zs - 1:
+            pass_on(w, slot(w, blk), blk, base + k, jnp.logical_and(cond, room), to)
+        c = remote(slot(w, blk), slot(w, blk), x_send.at[w, base + k], w_recv.at[w, blk], sp=mate)
+        pl.when(cond)(c.start)
+        held.append((cond, c))
+
+    def relay(w, k):
+        relay_one(w, k, True)
+        relay_one(w, k, False)
+
+    turn = 1 - 2 * (z // max(zs // 2, 1))
+
+    def column(d, side):
+        return lax.rem(z + turn * d + zs, zs) * inner + side
+
+    send_own(0)
+    send_own(1)
 
     i = lax.broadcasted_iota(jnp.int32, (rows, rows), 0)
     j = lax.broadcasted_iota(jnp.int32, (rows, rows), 1)
@@ -146,6 +171,10 @@
 
     only_owner(s, keep_slice)
 
+    if zs > 1:
+        relay(0, 1)
+        relay(1, 1)
+
     log_w = jnp.where(j <= i, run_col - run_row + li_row, far_below)
     loc_max = jnp.max(log_w, axis=1, keepdims=True)
     scores = dot(q_ref[...], k_ref[...], 1, 1) * scale * jnp.exp(log_w - loc_max)
@@ -210,6 +239,11 @@
             ).wait_recv()
 
         only_owner(src, got)
+
+    if zs > 2:
+        relay(0, 2)
+        relay(1, 2)
+    send_own(2)
 
     carried = run_col + m_in
     top = jnp.maximum(carried, loc_max)
@@ -225,45 +259,76 @@
     def part_of(a):
         return pl.ds(pl.multiple_of(a * part, part), part)
 
-    for d in range(1, m):
-        to = lax.rem(t + d, m)
-        mix_send[d - 1] = dot(gated[part_of(to), :], op_ref[...]).astype(bf16)
-        c = remote(mix_send.at[d - 1], mix_recv.at[d - 1], mx_send.at[d - 1], mx_recv.at[d - 1], tp=to)
+    c2 = lax.rem(t, 2)
+    y = lax.div(t, 2)
+    ys = m // 2
+    twin = y * 2 + (1 - c2)
+
+    def across(d, side):
+        return lax.rem(y + d, ys) * 2 + side
+
+    order = list(range(1, ys)) + [0]
+    pair = []
+    for d in order:
+        mix_send[d] = dot(gated[part_of(across(d, 1 - c2)), :], op_ref[...]).astype(bf16)
+        c = remote(mix_send.at[d], mix_pair.at[d], mx_send.at[d], mx_recv.at[d], tp=twin)
         c.start()
         waits.append(c)
-    mixed = dot(gated[part_of(t), :], op_ref[...]).astype(bf16).astype(f32)
-    for d in range(1, zs):
-        relay(0, d)
-    for d in range(1, m):
+        pair.append(c)
+    for d, pc in zip(order, pair):
+        mixed = dot(gated[part_of(across(d, c2)), :], op_ref[...]).astype(bf16).astype(f32)
+        pc.wait_recv()
+        mixed = mixed + mix_pair[d].astype(f32)
+        if d > 0:
+            mix_far[d - 1] = mixed.astype(bf16)
+            c = remote(
+                mix_far.at[d - 1], mix_recv.at[d - 1], my_send.at[d - 1], my_recv.at[d - 1],
+                tp=across(d, c2),
+            )
+            c.start()
+            waits.append(c)
+    for k in range(3, zs):
+        relay(0, k)
+        relay(1, k)
+    for d in range(1, ys):
         remote(
-            mix_send.at[d - 1], mix_recv.at[d - 1], mx_send.at[d - 1], mx_recv.at[d - 1], tp=t
+            mix_far.at[d - 1], mix_recv.at[d - 1], my_send.at[d - 1], my_recv.at[d - 1], tp=twin
         ).wait_recv()
         mixed = mixed + mix_recv[d - 1].astype(f32)
     mixed = mixed.astype(bf16).astype(f32)
     stream = (res_ref[...].astype(f32) + normalize(mixed, mg_ref[...])).astype(bf16)
     out_ref[...] = stream
     normed_all[part_of(t), :] = normalize(stream.astype(f32), pg_ref[...]).astype(bf16)
-    for d in range(1, m):
-        to = lax.rem(t + d, m)
+    def spread(src, sem, to):
         c = remote(
-            normed_all.at[part_of(t), :], normed_all.at[part_of(t), :],
-            ag_send.at[d - 1], ag_recv.at[t], tp=to,
+            normed_all.at[part_of(src), :], normed_all.at[part_of(src), :], sem, ag_recv.at[src], tp=to
         )
         c.start()
         waits.append(c)
-    for d in range(1, zs):
-        relay(1, d)
+
+    def landed(src):
+        remote(
+            normed_all.at[part_of(src), :], normed_all.at[part_of(src), :],
+            ag_send.at[0], ag_recv.at[src], tp=twin,
+        ).wait_recv()
+
+    for d in range(1, ys):
+        spread(t, ag_send.at[d], across(d, c2))
+    spread(t, ag_send.at[0], twin)
+    if zs > 1:
+        relay(2, 1)
+    for d in range(1, ys):
+        landed(across(d, c2))
+        spread(across(d, c2), ag_send.at[ys + d], twin)
+    for d in range(ys):
+        landed(across(d, 1 - c2))
+    if zs > 2:
+        relay(2, 2)
     own[0].wait()
     own[1].wait()
     for w in range(2):
         for d in range(zs):
-            arrived(w, mate_block(d))
-    for d in range(1, m):
-        src = lax.rem(t + d, m)
-        remote(
-            normed_all.at[part_of(src), :], normed_all.at[part_of(src), :],
-            ag_send.at[0], ag_recv.at[src], tp=src,
-        ).wait_recv()
+            arrived(w, column(d, 1 - x))
 
     hid = upg.shape[1]
     cols = 256 if hid % 256 == 0 else 128
@@ -317,47 +382,73 @@
     def chunk(c, kth):
         fs = pl.ds(pl.multiple_of(c * feats, feats), feats)
         ffn_send[:, fs] = dot(hidden[...], w_all[2, fs, :], 1, 1).astype(bf16)
-        for d in range(1, m):
-            to = lax.rem(t + d, m)
+        for d in order:
             cp = remote(
-                ffn_send.at[part_of(to), fs], ffn_recv.at[d - 1, :, fs],
-                f_send.at[d - 1, kth], f_recv.at[d - 1, c], tp=to,
+                ffn_send.at[part_of(across(d, 1 - c2)), fs], ffn_pair.at[d, :, fs],
+                f_send.at[d, kth], f_recv.at[d, c], tp=twin,
             )
             cp.start()
             waits.append(cp)
 
+    def paired(c, d):
+        fs = pl.ds(pl.multiple_of(c * feats, feats), feats)
+        remote(
+            ffn_pair.at[d, :, fs], ffn_pair.at[d, :, fs], f_send.at[d, 0], f_recv.at[d, c], tp=twin
+        ).wait_recv()
+
+    def far(c, kth):
+        fs = pl.ds(pl.multiple_of(c * feats, feats), feats)
+        for d in range(1, ys):
+            paired(c, d)
+            ffn_far[d - 1, :, fs] = (
+                ffn_send[part_of(across(d, c2)), fs].astype(f32) + ffn_pair[d, :, fs].astype(f32)
+            ).astype(bf16)
+            cp = remote(
+                ffn_far.at[d - 1, :, fs], ffn_recv.at[d - 1, :, fs],
+                g_send.at[d - 1, kth], g_recv.at[d - 1, c], tp=across(d, c2),
+            )
+            cp.start()
+            waits.append(cp)
+
+    for k in range(3, zs):
+        relay(2, k)
     own[2].wait()
+    ready = []
     if chunks == n:
-        chunk(s, 0)
-        for d in range(1, zs):
-            chunk(relay(2, d), d)
         for d in range(zs):
-            blk = mate_block(d)
-            arrived(2, blk)
-            chunk(blk, zs + d)
+            ready.append((column(d, x), False))
+        for d in range(zs):
+            ready.append((column(d, 1 - x), True))
     else:
-        for d in range(1, zs):
-            relay(2, d)
         for d in range(zs):
-            arrived(2, mate_block(d))
-        for c in range(chunks):
-            chunk(c, c)
+            arrived(2, column(d, 1 - x))
+        ready = [(c, False) for c in range(chunks)]
+    for kth, (c, late) in enumerate(ready):
+        if late:
+            arrived(2, c)
+        chunk(c, kth)
+        if kth > 0:
+            far(ready[kth - 1][0], kth - 1)
+    far(ready[-1][0], chunks - 1)
 
     for c in range(chunks):
         fs = pl.ds(c * feats, feats)
-        for d in range(1, m):
-            remote(
-                ffn_send.at[part_of(t), fs], ffn_recv.at[d - 1, :, fs],
-                f_send.at[d - 1, 0], f_recv.at[d - 1, c], tp=t,
+        paired(c, 0)
+        for d in range(1, ys):
+            remote(
+                ffn_far.at[d - 1, :, fs], ffn_recv.at[d - 1, :, fs],
+                g_send.at[d - 1, 0], g_recv.at[d - 1, c], tp=twin,
             ).wait_recv()
-    ffn = ffn_send[part_of(t), :].astype(f32)
-    for d in range(1, m):
+    ffn = ffn_send[part_of(t), :].astype(f32) + ffn_pair[0].astype(f32)
+    for d in range(1, ys):
         ffn = ffn + ffn_recv[d - 1].astype(f32)
     ffn = ffn.astype(bf16).astype(f32)
     out_ref[...] = (out_ref[...].astype(f32) + normalize(ffn, sg_ref[...])).astype(bf16)
 
     for c in waits:
         c.wait_send()
+    for cond, c in held:
+        pl.when(cond)(c.wait_send)
     for d in range(1, n):
         to = lax.rem(s + d, n)
 
@@ -399,6 +490,7 @@
     vm = pl.BlockSpec(memory_space=pltpu.VMEM)
     hbm = pl.BlockSpec(memory_space=pl.ANY)
     zs = n // 2
+    ys = m // 2
     return pl.pallas_call(
         functools.partial(kernel, n, m, owners, chunks),
         out_shape=jax.ShapeDtypeStruct(residual.shape, bf16),
@@ -412,8 +504,10 @@
             pltpu.VMEM((n, qk // owners, hv), bf16),
             pltpu.VMEM((qk, hv), bf16),
             pltpu.VMEM((rows, hv), bf16),
-            pltpu.VMEM((m - 1, part, width), bf16),
-            pltpu.VMEM((m - 1, part, width), bf16),
+            pltpu.VMEM((ys, part, width), bf16),
+            pltpu.VMEM((ys, part, width), bf16),
+            pltpu.VMEM((ys, part, width), bf16),
+            pltpu.VMEM((ys, part, width), bf16),
             pltpu.VMEM((rows, width), bf16),
             pltpu.VMEM((HALO + rows, hid), bf16),
             pltpu.VMEM((HALO + rows, hid), bf16),
@@ -421,10 +515,12 @@
             pltpu.VMEM((2, HALO, hid), bf16),
             pltpu.VMEM((rows, hid), bf16),
             pltpu.VMEM((rows, width), bf16),
-            pltpu.VMEM((m - 1, part, width), bf16),
+            pltpu.VMEM((ys, part, width), bf16),
+            pltpu.VMEM((ys, part, width), bf16),
+            pltpu.VMEM((ys, part, width), bf16),
             dma((3,)),
-            dma((3, zs)),
-            dma((3, zs)),
+            dma((3, 2 * zs)),
+            dma((3, 2 * zs)),
             dma((3, n)),
             dma((n,)),
             dma((n,)),
@@ -436,10 +532,14 @@
             dma((m,)),
             dma((m,)),
             dma((m,)),
+            dma((m,)),
+            dma((m,)),
             dma,
             dma,
-            dma((m, chunks)),
-            dma((m, chunks)),
+            dma((ys, chunks)),
+            dma((ys, chunks)),
+            dma((ys, chunks)),
+            dma((ys, chunks)),
         ],
         compiler_params=pltpu.CompilerParams(
             collective_id=0, has_side_effects=True, vmem_limit_bytes=64000000

time: 222 us -> 138 us (0.62)
  Pallas kernels: 217 us -> 135 us
    pallas_call x1, Pallas kernels: 217 us -> 135 us  [body(): pl.pallas_call(functools.partial(kernel, n, m, owners, chunks), out_shape...]
where the time goes in v2:
time: 138 us; the launch traced here: 137 us
  Pallas kernels  135 us (98%)
  local copies, waits for them, and re-layouts  1.88 us (1%)
    pallas_call x1, Pallas kernels, body(): pl.pallas_call(functools.partial(kernel, n, m, owners, chunks), out_shape...  135 us

profile of v2, /device:TPU:0, one launch (start us, length us, event | category | flops | bytes accessed | tf_op | source)
XLA Modules:
  0.0 136.5 jit_solution(11556606502502795181)
XLA Ops:
  0.0 134.6 %layer.1 = bf16[128,2048]{1,0:T(8,128)(2,1)} custom-call(bf16[512,256]{1,0:T(8,128)(2,1)} %q_ref.1, bf16[512,256]{1,0:T(8,128)(2,1)} %k_ref.1, bf16[512,512]{1,0:T(8,128)(2,1)} %v_ref.1, bf16[512,512]{1,0:T(8,128)(2,1)} %og_ref.1, f32[1,512]{1,0:T(1,128)} %ig_ref.1, f32[1,512]{1,0:T(1,128)} %fg_ref.1, bf16[128,2048]{1,0:T(8,128)(2,1)} %res_ref.1, ...), custom_call_target="tpu_custom_call" | custom-call | tf_op jit(solution)/shard_map/layer/pallas_call | solution.py:494
  134.6 1.9 %copy.18 = bf16[128,2048]{1,0:T(8,128)(2,1)} copy(bf16[128,2048]{1,0:T(8,128)(2,1)} %layer.1) | data formatting | bytes 1048576
